TPU v7x, 32 devices: a whole 2x2x4 slice. The times are simulated.
32 devices in a mesh: ep: 8 (over z, core), tp: 4 (over y, x).
Axes of the slice: x: 2, y: 2, z: 4, core: 2. Of those that a mesh axis runs over, the one named last changes fastest.
Arguments:
- mixer_input: bfloat16 [2048, 2048], P('ep'), may hold values from -6 to 6
- mixer_gain: float32 [2048], replicated, may hold values from 0.1 to 1.9
- query_weight: bfloat16 [2048, 2048], P(None, 'tp'), may hold values from -0.13258252 to 0.13258252
- key_weight: bfloat16 [2048, 1024], P(None, 'tp'), may hold values from -2.78423295 to 2.78423295
- value_weight: bfloat16 [2048, 1024], P(None, 'tp'), may hold values from -0.125 to 0.125
- output_weight: bfloat16 [2048, 2048], P(None, 'tp'), may hold values from -1 to 1
- sink_logit: float32 [32], P('tp'), may hold values from 2 to 7
- expert_input: bfloat16 [1024, 2048], P('ep'), may hold values from -6 to 6
- expert_gain: float32 [2048], replicated, may hold values from 0.1 to 1.9
- routes: int32 [1024, 4], P('ep'), may hold values from 0 to 7, all different within a row; in each aligned block of 128 rows (0 to 127, 128 to 255, ...) at most 128 rows name the same one
- route_logits: float32 [1024, 4], P('ep'), may hold values from -6 to 6
- gate_weight: bfloat16 [8, 2048, 2048], P('ep', None, 'tp'), may hold values from -0.375 to 0.375
- up_weight: bfloat16 [8, 2048, 2048], P('ep', None, 'tp'), may hold values from -0.375 to 0.375
- down_weight: bfloat16 [8, 2048, 2048], P('ep', None, 'tp'), may hold values from -0.03125 to 0.03125
Outputs:
- mixer_output: bfloat16 [2048, 2048], P('ep', 'tp')
- expert_output: bfloat16 [1024, 2048], P('ep', 'tp')
Inputs may be any that keep to these rules, and one draw needn't show every extreme that they name: `routes`: each token names 4 different experts. Among the 128 tokens of one index of ep (aligned blocks) no expert is named more than 128 times, and in some blocks one expert is named exactly 128 times.
All inputs are finite; a program needn't handle non-finite values.
Results may differ from a plain program's by a relative error of at most 0.0055.
The roundings to bfloat16 on the way count: a program that leaves them out, or rounds other values in their place, can miss the bound.
Values may be sent and summed in bfloat16 or wider, within the bound.
A program may use at most 64 MiB of HBM per device.

v0:
```python
import jax
import jax.numpy as jnp
from jax import lax
from jax.sharding import PartitionSpec as P

HEAD_DIM = 64
TOP_K = 4
WINDOW = 128
GRID_W = 64


EPSILON = 1e-06
LIMIT = 7.0
SLOPE = 1.702
BASE = 10000.0


def extended(shard, sides, width):
    for axis, dim in sides:
        devices, length = (lax.axis_size(axis), shard.shape[dim])
        up = [(i, (i + 1) % devices) for i in range(devices - 1)]
        down = [(j, i) for i, j in up]
        last = lax.slice_in_dim(shard, length - width, length, axis=dim)
        first = lax.slice_in_dim(shard, 0, width, axis=dim)
        before = lax.ppermute(last, axis, up)
        after = lax.ppermute(first, axis, down)
        shard = jnp.concatenate([before, shard, after], axis=dim)
    return shard


def normalize(rows, gain):
    values = rows.astype(jnp.float32)
    scaled = values * lax.rsqrt(jnp.mean(values * values, axis=-1, keepdims=True) + EPSILON)
    return (scaled * gain).astype(jnp.bfloat16)


def turn(values, cosine, sine):
    first, second = jnp.split(values, 2, axis=-1)
    cosine = cosine[:, None, :]
    sine = sine[:, None, :]
    return jnp.concatenate(
        [first * cosine - second * sine, second * cosine + first * sine], axis=-1
    )


def axial_rope(values, places):
    quarter = values.shape[-1] // 4
    frequency = BASE ** (-jnp.arange(quarter, dtype=jnp.float32) / quarter)
    row_angle = (places // GRID_W).astype(jnp.float32)[:, None] * frequency[None, :]
    column_angle = (places % GRID_W).astype(jnp.float32)[:, None] * frequency[None, :]
    row_part, column_part = jnp.split(values, 2, axis=-1)
    return jnp.concatenate(
        [
            turn(row_part, jnp.cos(row_angle), jnp.sin(row_angle)),
            turn(column_part, jnp.cos(column_angle), jnp.sin(column_angle)),
        ],
        axis=-1,
    )


def activate(gate, up):
    capped = jnp.minimum(gate, LIMIT)
    bounded = jnp.clip(up, -LIMIT, LIMIT)
    return (capped * jax.nn.sigmoid(SLOPE * capped) * (bounded + 1.0)).astype(jnp.bfloat16)


def add_product(piece, weight):
    return jnp.dot(piece, weight, preferred_element_type=jnp.float32)


def shards(
    mixer_input,
    mixer_gain,
    query_weight,
    key_weight,
    value_weight,
    output_weight,
    sink_logit,
    expert_input,
    expert_gain,
    routes,
    route_logits,
    gate_weight,
    up_weight,
    down_weight,
):
    tokens = mixer_input.shape[0]
    query_heads = query_weight.shape[1] // HEAD_DIM
    key_heads = key_weight.shape[1] // HEAD_DIM
    group = query_heads // key_heads
    blocks = tokens // WINDOW
    offset = lax.axis_index("ep") * tokens
    length = lax.axis_size("ep") * tokens
    places = offset + jnp.arange(tokens, dtype=jnp.int32)
    normed = normalize(mixer_input, mixer_gain)
    query = jnp.dot(normed, query_weight, preferred_element_type=jnp.float32).reshape(
        tokens, query_heads, HEAD_DIM
    )
    query = (
        axial_rope(query, places)
        .astype(jnp.bfloat16)
        .reshape(blocks, WINDOW, key_heads, group, HEAD_DIM)
    )
    keys = jnp.dot(normed, key_weight, preferred_element_type=jnp.float32).reshape(
        tokens, key_heads, HEAD_DIM
    )
    keys = axial_rope(keys, places).astype(jnp.bfloat16).reshape(tokens, key_heads * HEAD_DIM)
    values = jnp.dot(normed, value_weight, preferred_element_type=jnp.float32).astype(jnp.bfloat16)
    stacked = jnp.concatenate([keys, values], axis=1)
    widened = extended(stacked, (("ep", 0),), WINDOW)
    framed = widened.reshape(blocks + 2, WINDOW, 2, key_heads, HEAD_DIM)
    nearby = jnp.concatenate([framed[:-2], framed[1:-1], framed[2:]], axis=1)
    scores = jnp.einsum(
        "nqgrd,nkgd->ngrqk", query, nearby[:, :, 0], preferred_element_type=jnp.float32
    ) * HEAD_DIM ** (-0.5)
    query_place = places.reshape(blocks, WINDOW)
    key_place = (
        offset
        + (jnp.arange(blocks, dtype=jnp.int32)[:, None] - 1) * WINDOW
        + jnp.arange(3 * WINDOW, dtype=jnp.int32)[None, :]
    )
    allowed = (
        (jnp.abs(query_place[:, :, None] - key_place[:, None, :]) <= WINDOW)
        & (key_place[:, None, :] >= 0)
        & (key_place[:, None, :] < length)
    )
    scores = jnp.where(allowed[:, None, None], scores, -1e30)
    sinks = sink_logit.reshape(key_heads, group)[None, :, :, None]
    top = jnp.maximum(jnp.max(scores, axis=-1), sinks)
    weights = jnp.exp(scores - top[..., None])
    denominator = jnp.sum(weights, axis=-1) + jnp.exp(sinks - top)
    shares = (weights / denominator[..., None]).astype(jnp.bfloat16)
    mixed = jnp.einsum(
        "ngrqk,nkgd->nqgrd", shares, nearby[:, :, 1], preferred_element_type=jnp.float32
    )
    mixed = mixed.astype(jnp.bfloat16).reshape(tokens, query_heads * HEAD_DIM)
    experts = lax.axis_size("ep")
    rows_here = expert_input.shape[0]
    capacity = 2 * rows_here * TOP_K // experts
    expert_normed = normalize(expert_input, expert_gain)
    chances = jax.nn.softmax(route_logits, axis=-1)
    chosen = routes.reshape(-1)
    marks = (chosen[:, None] == jnp.arange(experts, dtype=jnp.int32)[None, :]).astype(jnp.int32)
    earlier = jnp.sum((jnp.cumsum(marks, axis=0) - marks) * marks, axis=1)
    target = chosen * capacity + earlier
    source = (
        jnp.full((experts * capacity,), rows_here, jnp.int32)
        .at[target]
        .set(jnp.arange(chosen.shape[0], dtype=jnp.int32) // TOP_K)
    )
    padded = jnp.concatenate(
        [expert_normed, jnp.zeros((1, expert_normed.shape[1]), jnp.bfloat16)], axis=0
    )
    down_local = down_weight[0]
    gate_local = gate_weight[0]
    up_local = up_weight[0]
    width = padded.shape[1] // lax.axis_size("tp")
    own = lax.dynamic_slice_in_dim(padded, lax.axis_index("tp") * width, width, 1)
    outgoing = own[source].reshape(experts, capacity, width)
    received = lax.all_to_all(outgoing, "ep", split_axis=0, concat_axis=0, tiled=True)
    flat = received.reshape(experts * capacity, width)
    head_piece = lax.all_gather(mixed, "tp", axis=1, tiled=True)
    feature_piece = lax.all_gather(flat, "tp", axis=1, tiled=True)
    mixer_total = add_product(head_piece, output_weight)
    gate = add_product(feature_piece, gate_local)
    up = add_product(feature_piece, up_local)
    hidden = activate(gate, up)
    result = add_product(lax.all_gather(hidden, "tp", axis=1, tiled=True), down_local)
    result = result.astype(jnp.bfloat16).reshape(experts, capacity, down_local.shape[1])
    returned = lax.all_to_all(result, "ep", split_axis=0, concat_axis=0, tiled=True)
    mixer_output = mixer_total.astype(jnp.bfloat16)
    results = returned.reshape(experts * capacity, returned.shape[2])
    picked = results[target].astype(jnp.float32).reshape(rows_here, TOP_K, returned.shape[2])
    expert_output = jnp.sum(picked * chances[:, :, None], axis=1).astype(jnp.bfloat16)
    return (mixer_output, expert_output)


def solution(mesh):
    return jax.shard_map(
        shards,
        mesh=mesh,
        in_specs=(
            P("ep", None),
            P(),
            P(None, "tp"),
            P(None, "tp"),
            P(None, "tp"),
            P(None, "tp"),
            P("tp"),
            P("ep", None),
            P(),
            P("ep", None),
            P("ep", None),
            P("ep", None, "tp"),
            P("ep", None, "tp"),
            P("ep", None, "tp"),
        ),
        out_specs=(P("ep", "tp"), P("ep", "tp")),
        check_vma=False,
    )
```

profile of v0, /device:TPU:0, one launch (start us, length us, event | category | flops | bytes accessed | tf_op | source)
XLA Modules:
  0.0 214.6 jit_solution(16968832232059653629)
XLA Ops:
  9.1 1.2 fusion.19
  10.3 1.1 reduce-window.6
  12.0 2.4 %scatter_custom_fusion = s32[1024]{0:T(1024)S(1)} fusion(s32[512]{0:T(512)S(1)} %bitcast.98, s32[512]{0:T(512)S(1)} %add_select_fusion, s32[]{:T(128)} %constant.101.clone.1), kind=kCustom, calls=%fused_computation.95 | custom fusion | bytes 4100 | tf_op jit(solution)/shard_map/scatter | solution.py:149
  14.5 1.2 fusion.21
  15.8 4.0 %gather_fusion = bf16[1024,512]{1,0:T(8,128)(2,1)S(1)} fusion(bf16[129,512]{1,0:T(8,128)(2,1)S(1)} %pad_dynamic-slice_fusion, s32[1024]{0:T(1024)S(1)} %fusion.37), kind=kCustom, calls=%fused_computation | custom fusion | bytes 2101248 | tf_op jit(solution)/shard_map/gather | solution.py:159
  19.7 32.8 %all_to_all.10 = bf16[8,128,512]{2,1,0:T(8,128)(2,1)} all-to-all(bf16[8,128,512]{2,1,0:T(8,128)(2,1)S(1)} %bitcast.89), channel_id=1, replica_groups=mesh['ep'=8,'tp'=4] {'ep'}, dimensions={0} | all-to-all | bytes 2097152 | tf_op jit(solution)/shard_map/all_to_all | solution.py:160
  52.6 51.5 %all-gather.6.cloned.1.call-done = bf16[1024,2048]{1,0:T(8,128)(2,1)} async-done(((bf16[1024,512]{1,0:T(8,128)(2,1)}), bf16[1024,2048]{1,0:T(8,128)(2,1)}) %all-gather.6.cloned.1.call-update) | async-done | bytes 4194320 | tf_op jit(solution)/shard_map/all_gather | solution.py:163
  104.1 4.7 %fusion.7 = f32[1024,512]{1,0:T(8,128)S(1)} fusion(bf16[1024,2048]{1,0:T(8,128)(2,1)} %all-gather.6.cloned.1.call-done, bf16[1,2048,512]{2,1,0:T(8,128)(2,1)S(1)} %copy-done), kind=kOutput, calls=%fused_computation.15 | convolution fusion | flops 2147483648 | bytes 8388608 | tf_op jit(solution)/shard_map/dot_general | solution.py:68
  108.8 3.8 %multiply_convert_fusion = bf16[1024,512]{1,0:T(8,128)(2,1)} fusion(f32[1024,512]{1,0:T(8,128)S(1)} %fusion.7, bf16[1024,2048]{1,0:T(8,128)(2,1)S(1)} %copy-done.4, bf16[1,2048,512]{2,1,0:T(8,128)(2,1)S(1)} %copy-done.5), kind=kOutput, calls=%fused_computation.19 | convolution fusion | flops 2152726528 | bytes 9437184 | tf_op jit(solution)/shard_map/dot_general | solution.py:68
  113.4 1.9 fusion.56
  116.8 2.2 %collective-permute-start = (bf16[128,512]{0,1:T(8,128)(2,1)}, bf16[128,512]{0,1:T(8,128)(2,1)}, u32[]{:S(2)}, u32[]{:S(2)}) collective-permute-start(bf16[128,512]{0,1:T(8,128)(2,1)} %get-tuple-element.16), channel_id=1, source_target_pairs={{0,4},{4,8},{8,12},{12,16},{16,20},{20,24},{24,28},{1,5},{5,9},{9,... | collective-permute-start | bytes 393224 | tf_op jit(solution)/shard_map/ppermute | solution.py:25
  119.0 1.6 collective-permute-start.1
  120.6 1.1 fusion.53
  125.1 1.0 pad_maximum_fusion.1
  126.6 1.6 fusion.1
  131.1 34.2 %all-gather.8.cloned.1.call-done = bf16[1024,2048]{1,0:T(8,128)(2,1)} async-done(((bf16[1024,512]{1,0:T(8,128)(2,1)}), bf16[1024,2048]{1,0:T(8,128)(2,1)}) %all-gather.8.cloned.1.call-update) | async-done | bytes 4194320 | tf_op jit(solution)/shard_map/all_gather | solution.py:168
  165.3 6.2 %fusion.14 = bf16[1024,512]{1,0:T(8,128)(2,1)} fusion(bf16[1024,2048]{1,0:T(8,128)(2,1)} %all-gather.8.cloned.1.call-done, bf16[1,2048,512]{2,1,0:T(8,128)(2,1)} %param.27), kind=kOutput, calls=%fused_computation.21 | convolution fusion | flops 2148007936 | bytes 7340032 | tf_op jit(solution)/shard_map/dot_general | solution.py:68
  171.5 4.7 %all-to-all-start.1 = ((bf16[8,128,512]{2,1,0:T(8,128)(2,1)}), bf16[8,128,512]{2,1,0:T(8,128)(2,1)S(1)}, u32[]{:S(2)}, u32[]{:S(2)}) async-start(bf16[8,128,512]{2,1,0:T(8,128)(2,1)} %bitcast.93), calls=%async_computation.1 | async-start | bytes 2097152 | tf_op jit(solution)/shard_map/all_to_all | solution.py:170
  176.4 17.9 %all-gather.4.cloned.1.call-done = bf16[256,2048]{0,1:T(8,128)(2,1)} async-done(((bf16[256,512]{0,1:T(8,128)(2,1)}), bf16[256,2048]{0,1:T(8,128)(2,1)}) %all-gather.4.cloned.1.call-update) | async-done | bytes 1048592 | tf_op jit(solution)/shard_map/all_gather | solution.py:162
  194.2 3.3 %convolution_convert_fusion = bf16[256,512]{1,0:T(8,128)(2,1)} fusion(bf16[256,2048]{0,1:T(8,128)(2,1)} %all-gather.4.cloned.1.call-done, bf16[2048,512]{1,0:T(8,128)(2,1)} %param.19), kind=kOutput, calls=%fused_computation.24 | convolution fusion | flops 537001984 | bytes 3407872 | tf_op jit(solution)/shard_map/dot_general | solution.py:68
  197.6 5.2 %all-to-all-done.1 = bf16[8,128,512]{2,1,0:T(8,128)(2,1)S(1)} async-done(((bf16[8,128,512]{2,1,0:T(8,128)(2,1)}), bf16[8,128,512]{2,1,0:T(8,128)(2,1)S(1)}, u32[]{:S(2)}, u32[]{:S(2)}) %all-to-all-start.1) | async-done | bytes 1048608 | tf_op jit(solution)/shard_map/all_to_all | solution.py:170
  202.8 2.6 %gather_fusion.1 = bf16[512,512]{1,0:T(8,128)(2,1)} fusion(bf16[1024,512]{1,0:T(8,128)(2,1)S(1)} %bitcast.88, s32[1024]{0:T(1024)S(1)} %pad_clamp_fusion), kind=kCustom, calls=%fused_computation.1 | custom fusion | bytes 1050624 | tf_op jit(solution)/shard_map/gather | solution.py:173
  205.4 1.4 reshape.338
  206.7 1.4 multiply_reduce_fusion
  (83 shorter events, 11.5 us)
Async XLA Ops:
  7.2 97.0 %copy-start = (bf16[1,2048,512]{2,1,0:T(8,128)(2,1)S(1)}, bf16[1,2048,512]{2,1,0:T(8,128)(2,1)}, u32[]{:S(2)}) copy-start(bf16[1,2048,512]{2,1,0:T(8,128)(2,1)} %param.26) | copy-start | bytes 6291460
  7.2 96.9 %all-gather.6.cloned.1.call-start = ((), (), s32[]{:S(2)}) async-start(), calls=%async_computation.3 | async-start | bytes 5242880 | tf_op jit(solution)/shard_map/all_gather | solution.py:163
  52.6 112.7 %all-gather.8.cloned.1.call-start = ((), (), s32[]{:S(2)}) async-start(), calls=%async_computation.4 | async-start | bytes 5242880 | tf_op jit(solution)/shard_map/all_gather | solution.py:168
  104.1 4.7 %copy-start.4 = (bf16[1024,2048]{1,0:T(8,128)(2,1)S(1)}, bf16[1024,2048]{1,0:T(8,128)(2,1)}, u32[]{:S(2)}) copy-start(bf16[1024,2048]{1,0:T(8,128)(2,1)} %all-gather.6.cloned.1.call-done) | copy-start | bytes 12582916
  104.1 4.7 %copy-start.5 = (bf16[1,2048,512]{2,1,0:T(8,128)(2,1)S(1)}, bf16[1,2048,512]{2,1,0:T(8,128)(2,1)}, u32[]{:S(2)}) copy-start(bf16[1,2048,512]{2,1,0:T(8,128)(2,1)} %param.25) | copy-start | bytes 6291460
  108.8 4.0 %copy-start.1 = (bf16[256,2048]{1,0:T(8,128)(2,1)S(1)}, bf16[256,2048]{1,0:T(8,128)(2,1)}, u32[]{:S(2)}) copy-start(bf16[256,2048]{1,0:T(8,128)(2,1)} %param.14) | copy-start | bytes 3145732
  112.7 0.7 copy-start.8
  112.7 81.5 %all-gather.4.cloned.1.call-start = ((), (), s32[]{:S(2)}) async-start(), calls=%async_computation.2 | async-start | bytes 1310720 | tf_op jit(solution)/shard_map/all_gather | solution.py:162
  113.1 2.3 %copy-start.7 = (bf16[2048,256]{1,0:T(8,128)(2,1)S(1)}, bf16[2048,256]{1,0:T(8,128)(2,1)}, u32[]{:S(2)}) copy-start(bf16[2048,256]{1,0:T(8,128)(2,1)} %param.18) | copy-start | bytes 3145732
  115.3 5.3 %copy-start.6 = (bf16[2048,512]{1,0:T(8,128)(2,1)S(1)}, bf16[2048,512]{1,0:T(8,128)(2,1)}, u32[]{:S(2)}) copy-start(bf16[2048,512]{1,0:T(8,128)(2,1)} %param.16) | copy-start | bytes 6291460
  116.8 8.3 %collective-permute-start = (bf16[128,512]{0,1:T(8,128)(2,1)}, bf16[128,512]{0,1:T(8,128)(2,1)}, u32[]{:S(2)}, u32[]{:S(2)}) collective-permute-start(bf16[128,512]{0,1:T(8,128)(2,1)} %get-tuple-element.16), channel_id=1, source_target_pairs={{0,4},{4,8},{8,12},{12,16},{16,20},{20,24},{24,28},{1,5},{5,9},{9,... | collective-permute-start | bytes 393224 | tf_op jit(solution)/shard_map/ppermute | solution.py:25
  119.0 5.4 %copy-start.3 = (f32[8]{0:T(128)S(1)}, f32[8]{0:T(128)}, u32[]{:S(2)}) copy-start(f32[8]{0:T(128)} %param.20) | copy-start | bytes 100
  119.0 6.1 %collective-permute-start.1 = (bf16[128,512]{0,1:T(8,128)(2,1)}, bf16[128,512]{0,1:T(8,128)(2,1)}, u32[]{:S(2)}, u32[]{:S(2)}) collective-permute-start(bf16[128,512]{0,1:T(8,128)(2,1)} %get-tuple-element.15), channel_id=1, source_target_pairs={{4,0},{8,4},{12,8},{16,12},{20,16},{24,20},{28,24},{5,1},{9,5},{13... | collective-permute-start | bytes 393224 | tf_op jit(solution)/shard_map/ppermute | solution.py:26
  171.5 4.7 %copy-start.2 = (f32[128,4]{0,1:T(4,128)S(1)}, f32[128,4]{0,1:T(4,128)}, u32[]{:S(2)}) copy-start(f32[128,4]{0,1:T(4,128)} %param.24) | copy-start | bytes 6148
  171.5 31.3 %all-to-all-start.1 = ((bf16[8,128,512]{2,1,0:T(8,128)(2,1)}), bf16[8,128,512]{2,1,0:T(8,128)(2,1)S(1)}, u32[]{:S(2)}, u32[]{:S(2)}) async-start(bf16[8,128,512]{2,1,0:T(8,128)(2,1)} %bitcast.93), calls=%async_computation.1 | async-start | bytes 2097152 | tf_op jit(solution)/shard_map/all_to_all | solution.py:170
Sparse Core Ops, SparseCore 0:
  52.7 51.3 all-gather.5
  112.8 52.4 all-gather.7
  167.7 26.4 all-gather.3
where the time goes:
time: 215 us
  waiting for transfers between devices  109 us (51%)
  blocking collectives  32.8 us (15%)
  matrix products  24.2 us (11%)
  local copies, waits for them, and re-layouts  16.3 us (8%)
  between operations  14.1 us (7%)
  other arithmetic  9.73 us (5%)
  starting transfers between devices  8.66 us (4%)
    all_gather x1, waiting for transfers between devices, shards(): feature_piece = lax.all_gather(flat, 'tp', axis=1, tiled=True)  51.5 us
    all_gather x1, waiting for transfers between devices, shards(): lax.all_gather(hidden, 'tp', axis=1, tiled=True)  34.2 us
    all_to_all x1, blocking collectives, shards(): lax.all_to_all(outgoing, 'ep', split_axis=0, concat_axis=0, tiled=True)  32.8 us
    dot_general x4, matrix products, add_product(): return jnp.dot(piece, weight, preferred_element_type=jnp.float32)  18 us
    all_gather x1, waiting for transfers between devices, shards(): head_piece = lax.all_gather(mixed, 'tp', axis=1, tiled=True)  17.9 us
    all_to_all x1, waiting for transfers between devices, shards(): lax.all_to_all(result, 'ep', split_axis=0, concat_axis=0, tiled=True)  5.17 us
    all_to_all x1, starting transfers between devices, shards(): lax.all_to_all(result, 'ep', split_axis=0, concat_axis=0, tiled=True)  4.74 us
  transfers between devices with their start and end apart: 6, of which 4 were waited for; matrix products, arithmetic and copies ran while one was open for 11% of the time, Pallas kernels for 0%

commit v1 on v0

--- a/solution.py
+++ b/solution.py
@@ -1,6 +1,10 @@
+import functools
+
 import jax
 import jax.numpy as jnp
 from jax import lax
+from jax.experimental import pallas as pl
+from jax.experimental.pallas import tpu as pltpu
 from jax.sharding import PartitionSpec as P
 
 HEAD_DIM = 64
@@ -64,8 +68,240 @@
     return (capped * jax.nn.sigmoid(SLOPE * capped) * (bounded + 1.0)).astype(jnp.bfloat16)
 
 
-def add_product(piece, weight):
-    return jnp.dot(piece, weight, preferred_element_type=jnp.float32)
+def remote(src, dst, sent, landed, ep, tp):
+    return pltpu.make_async_remote_copy(
+        src_ref=src,
+        dst_ref=dst,
+        send_sem=sent,
+        recv_sem=landed,
+        device_id=(ep, tp),
+        device_id_type=pl.DeviceIdType.MESH,
+    )
+
+
+def exchange(
+    n,
+    t,
+    x_ref,
+    gain_ref,
+    share_ref,
+    mixed_ref,
+    wo_hbm,
+    wg_hbm,
+    wu_hbm,
+    wd_hbm,
+    mixer_out,
+    expert_out,
+    tokens,
+    hidden,
+    heads,
+    result,
+    returned,
+    wo,
+    wg,
+    wu,
+    wd,
+    local_sem,
+    token_recv,
+    far_send,
+    near_send,
+    core_send,
+    hidden_send,
+    hidden_recv,
+    head_send,
+    head_recv,
+    result_send,
+    result_recv,
+):
+    ep, tp = lax.axis_index("ep"), lax.axis_index("tp")
+    chips = n // 2
+    z, core = ep // 2, ep % 2
+    step = 1 - 2 * core
+    partner = 2 * z + 1 - core
+    rows = x_ref.shape[0]
+    pair = 2 * rows
+    part = wg.shape[1]
+    far, near = chips // 2, chips - 1 - chips // 2
+
+    def chip(hops):
+        return lax.rem(z + hops * step + 2 * chips, chips)
+
+    def block(buffer, index, size):
+        return buffer.at[pl.ds(pl.multiple_of(index * size, size), size)]
+
+    loads = [
+        pltpu.make_async_copy(a, b, local_sem.at[i])
+        for i, (a, b) in enumerate(((wg_hbm, wg), (wu_hbm, wu), (wo_hbm, wo), (wd_hbm, wd)))
+    ]
+    for load in loads:
+        load.start()
+
+    barrier = pltpu.get_barrier_semaphore()
+    for k in range(1, n):
+        pl.semaphore_signal(
+            barrier,
+            inc=1,
+            device_id=(lax.rem(ep + k, n), tp),
+            device_id_type=pl.DeviceIdType.MESH,
+        )
+    for k in range(1, t):
+        pl.semaphore_signal(
+            barrier,
+            inc=1,
+            device_id=(ep, lax.rem(tp + k, t)),
+            device_id_type=pl.DeviceIdType.MESH,
+        )
+    tokens[pl.ds(pl.multiple_of(ep * rows, rows), rows), :] = normalize(x_ref[...], gain_ref[...])
+    pl.semaphore_wait(barrier, n + t - 2)
+
+    def token_copy(slot, sent, target):
+        piece = block(tokens, slot, rows)
+        return remote(piece, piece, sent, token_recv.at[slot], target, tp)
+
+    def forward_far(hop):
+        return token_copy(2 * chip(-hop) + core, far_send.at[hop], 2 * chip(1) + core)
+
+    def forward_near(hop):
+        return token_copy(2 * chip(hop) + core, near_send.at[hop], 2 * chip(-1) + core)
+
+    def forward_core(hops):
+        place = chip(hops)
+        return token_copy(2 * place + core, core_send.at[place], partner)
+
+    def token_wait(slot):
+        token_copy(slot, core_send.at[0], partner).wait_recv()
+
+    if far > 0:
+        forward_far(0).start()
+    if near > 0:
+        forward_near(0).start()
+    forward_core(0).start()
+
+    def head_copy(source, k):
+        return remote(
+            mixed_ref, heads.at[source], head_send.at[k], head_recv.at[source], ep, lax.rem(tp + k, t)
+        )
+
+    for k in range(1, t):
+        head_copy(tp, k).start()
+    heads[tp] = mixed_ref[...]
+
+    def hidden_copy(source, place, k):
+        piece = block(hidden.at[source], place, pair)
+        return remote(
+            piece,
+            piece,
+            hidden_send.at[k, place],
+            hidden_recv.at[source, place],
+            ep,
+            lax.rem(tp + k, t),
+        )
+
+    def first_half(place):
+        token_wait(2 * place + 1 - core)
+        inside = pl.ds(pl.multiple_of(place * pair, pair), pair)
+        span = min(256, part)
+        for start in range(0, part, span):
+            cut = slice(start, start + span)
+            gate = jnp.dot(tokens[inside, :], wg[:, cut], preferred_element_type=jnp.float32)
+            up = jnp.dot(tokens[inside, :], wu[:, cut], preferred_element_type=jnp.float32)
+            hidden[tp, inside, cut] = activate(gate, up)
+        for k in range(1, t):
+            hidden_copy(tp, place, k).start()
+
+    loads[0].wait()
+    loads[1].wait()
+    first_half(z)
+    for hop in range(1, far + 1):
+        token_wait(2 * chip(-hop) + core)
+        if hop < far:
+            forward_far(hop).start()
+        forward_core(-hop).start()
+        if hop <= near:
+            token_wait(2 * chip(hop) + core)
+            if hop < near:
+                forward_near(hop).start()
+            forward_core(hop).start()
+
+            def both(k, carry, hop=hop):
+                first_half(chip((2 * k - 1) * hop))
+                return carry
+
+            lax.fori_loop(0, 2, both, 0)
+        else:
+            first_half(chip(-hop))
+
+    loads[2].wait()
+    for k in range(1, t):
+        head_copy(lax.rem(tp + k, t), k).wait_recv()
+    total = jnp.dot(heads[0], wo[0:part, :], preferred_element_type=jnp.float32)
+    for k in range(1, t):
+        total += jnp.dot(
+            heads[k], wo[k * part : (k + 1) * part, :], preferred_element_type=jnp.float32
+        )
+    mixer_out[...] = total.astype(jnp.bfloat16)
+
+    loads[3].wait()
+
+    def result_copy(source, owner):
+        return remote(
+            block(result, owner, rows),
+            returned.at[source],
+            result_send.at[owner],
+            result_recv.at[source],
+            owner,
+            tp,
+        )
+
+    def second_half(i, carry):
+        hop = (i + 1) // 2
+        place = chip(hop * (2 * ((i + 1) % 2) - 1))
+        inside = pl.ds(pl.multiple_of(place * pair, pair), pair)
+        for k in range(1, t):
+            hidden_copy(lax.rem(tp + k, t), place, k).wait_recv()
+        total = jnp.dot(hidden[0, inside, :], wd[0:part, :], preferred_element_type=jnp.float32)
+        for k in range(1, t):
+            total += jnp.dot(
+                hidden[k, inside, :],
+                wd[k * part : (k + 1) * part, :],
+                preferred_element_type=jnp.float32,
+            )
+        result[inside, :] = total.astype(jnp.bfloat16)
+
+        @pl.when(i == 0)
+        def _():
+            result_copy(ep, partner).start()
+            returned[ep] = result[pl.ds(pl.multiple_of(ep * rows, rows), rows), :]
+
+        @pl.when(i > 0)
+        def _():
+            result_copy(ep, 2 * place + core).start()
+            result_copy(ep, 2 * place + 1 - core).start()
+
+        return carry
+
+    lax.fori_loop(0, chips, second_half, 0)
+
+    for k in range(1, n):
+        other = lax.rem(ep + k, n)
+        result_copy(other, other).wait_recv()
+    total = returned[0].astype(jnp.float32) * share_ref[:, 0:1]
+    for e in range(1, n):
+        total += returned[e].astype(jnp.float32) * share_ref[:, e : e + 1]
+    expert_out[...] = total.astype(jnp.bfloat16)
+
+    for hop in range(far):
+        forward_far(hop).wait_send()
+    for hop in range(near):
+        forward_near(hop).wait_send()
+    for hop in range(chips):
+        forward_core(hop).wait_send()
+    for k in range(1, t):
+        head_copy(tp, k).wait_send()
+        for place in range(chips):
+            hidden_copy(tp, place, k).wait_send()
+    for k in range(1, n):
+        result_copy(ep, lax.rem(ep + k, n)).wait_send()
 
 
 def shards(
@@ -135,44 +371,60 @@
     )
     mixed = mixed.astype(jnp.bfloat16).reshape(tokens, query_heads * HEAD_DIM)
     experts = lax.axis_size("ep")
-    rows_here = expert_input.shape[0]
-    capacity = 2 * rows_here * TOP_K // experts
-    expert_normed = normalize(expert_input, expert_gain)
+    parts = lax.axis_size("tp")
+    rows_here, width = expert_input.shape
+    part = gate_weight.shape[2]
     chances = jax.nn.softmax(route_logits, axis=-1)
-    chosen = routes.reshape(-1)
-    marks = (chosen[:, None] == jnp.arange(experts, dtype=jnp.int32)[None, :]).astype(jnp.int32)
-    earlier = jnp.sum((jnp.cumsum(marks, axis=0) - marks) * marks, axis=1)
-    target = chosen * capacity + earlier
-    source = (
-        jnp.full((experts * capacity,), rows_here, jnp.int32)
-        .at[target]
-        .set(jnp.arange(chosen.shape[0], dtype=jnp.int32) // TOP_K)
-    )
-    padded = jnp.concatenate(
-        [expert_normed, jnp.zeros((1, expert_normed.shape[1]), jnp.bfloat16)], axis=0
-    )
-    down_local = down_weight[0]
-    gate_local = gate_weight[0]
-    up_local = up_weight[0]
-    width = padded.shape[1] // lax.axis_size("tp")
-    own = lax.dynamic_slice_in_dim(padded, lax.axis_index("tp") * width, width, 1)
-    outgoing = own[source].reshape(experts, capacity, width)
-    received = lax.all_to_all(outgoing, "ep", split_axis=0, concat_axis=0, tiled=True)
-    flat = received.reshape(experts * capacity, width)
-    head_piece = lax.all_gather(mixed, "tp", axis=1, tiled=True)
-    feature_piece = lax.all_gather(flat, "tp", axis=1, tiled=True)
-    mixer_total = add_product(head_piece, output_weight)
-    gate = add_product(feature_piece, gate_local)
-    up = add_product(feature_piece, up_local)
-    hidden = activate(gate, up)
-    result = add_product(lax.all_gather(hidden, "tp", axis=1, tiled=True), down_local)
-    result = result.astype(jnp.bfloat16).reshape(experts, capacity, down_local.shape[1])
-    returned = lax.all_to_all(result, "ep", split_axis=0, concat_axis=0, tiled=True)
-    mixer_output = mixer_total.astype(jnp.bfloat16)
-    results = returned.reshape(experts * capacity, returned.shape[2])
-    picked = results[target].astype(jnp.float32).reshape(rows_here, TOP_K, returned.shape[2])
-    expert_output = jnp.sum(picked * chances[:, :, None], axis=1).astype(jnp.bfloat16)
-    return (mixer_output, expert_output)
+    named = routes[:, :, None] == jnp.arange(experts, dtype=jnp.int32)[None, None, :]
+    expert_share = jnp.sum(jnp.where(named, chances[:, :, None], 0.0), axis=1)
+    vmem = pl.BlockSpec(memory_space=pltpu.VMEM)
+    anywhere = pl.BlockSpec(memory_space=pl.ANY)
+    chips = experts // 2
+    dma = pltpu.SemaphoreType.DMA
+    columns = down_weight.shape[2]
+    return pl.pallas_call(
+        functools.partial(exchange, experts, parts),
+        out_shape=(
+            jax.ShapeDtypeStruct((tokens, output_weight.shape[1]), jnp.bfloat16),
+            jax.ShapeDtypeStruct((rows_here, columns), jnp.bfloat16),
+        ),
+        in_specs=[vmem] * 4 + [anywhere] * 4,
+        out_specs=(vmem, vmem),
+        scratch_shapes=[
+            pltpu.VMEM((experts * rows_here, width), jnp.bfloat16),
+            pltpu.VMEM((parts, experts * rows_here, part), jnp.bfloat16),
+            pltpu.VMEM((parts, tokens, mixed.shape[1]), jnp.bfloat16),
+            pltpu.VMEM((experts * rows_here, columns), jnp.bfloat16),
+            pltpu.VMEM((experts, rows_here, columns), jnp.bfloat16),
+            pltpu.VMEM(output_weight.shape, jnp.bfloat16),
+            pltpu.VMEM(gate_weight.shape[1:], jnp.bfloat16),
+            pltpu.VMEM(up_weight.shape[1:], jnp.bfloat16),
+            pltpu.VMEM(down_weight.shape[1:], jnp.bfloat16),
+            dma((4,)),
+            dma((experts,)),
+            dma((chips,)),
+            dma((chips,)),
+            dma((chips,)),
+            dma((parts, chips)),
+            dma((parts, chips)),
+            dma((parts,)),
+            dma((parts,)),
+            dma((experts,)),
+            dma((experts,)),
+        ],
+        compiler_params=pltpu.CompilerParams(
+            collective_id=0, has_side_effects=True, vmem_limit_bytes=60 * 1024 * 1024
+        ),
+    )(
+        expert_input,
+        expert_gain.reshape(1, -1),
+        expert_share,
+        mixed,
+        output_weight,
+        gate_weight[0],
+        up_weight[0],
+        down_weight[0],
+    )
 
 
 def solution(mesh):

time: 215 us -> 113 us (0.53)
  waiting for transfers between devices: 109 us -> 0.01 us
  Pallas kernels: 0 us -> 85.6 us
  blocking collectives: 32.8 us -> 0 us
  matrix products: 24.2 us -> 6.54 us
  between operations: 14.1 us -> 0.91 us
  local copies, waits for them, and re-layouts: 16.3 us -> 9.71 us
  other arithmetic: 9.73 us -> 5.29 us
  starting transfers between devices: 8.66 us -> 4.32 us
    all_gather x3 -> x0, waiting for transfers between devices: 104 us -> none  [the longest x1 51.5 us: shards(): feature_piece = lax.all_gather(flat, 'tp', axis=1, tiled=True)]
    pallas_call x0 -> x1, Pallas kernels: none -> 85.6 us  [shards(): pl.pallas_call(functools.partial(exchange, experts, parts), out_shape=(ja...]
    all_to_all x1 -> x0, blocking collectives: 32.8 us -> none  [shards(): lax.all_to_all(outgoing, 'ep', split_axis=0, concat_axis=0, tiled=True)]
    dot_general x4 -> x0, matrix products: 18 us -> none  [add_product(): return jnp.dot(piece, weight, preferred_element_type=jnp.float32)]
    gather x2 -> x0, local copies, waits for them, and re-layouts: 6.58 us -> none  [the longest x1 3.97 us: shards(): outgoing = own[source].reshape(experts, capacity, width)]
    all_to_all x1 -> x0, waiting for transfers between devices: 5.17 us -> none  [shards(): lax.all_to_all(result, 'ep', split_axis=0, concat_axis=0, tiled=True)]
    all_to_all x1 -> x0, starting transfers between devices: 4.74 us -> none  [shards(): lax.all_to_all(result, 'ep', split_axis=0, concat_axis=0, tiled=True)]
    unnamed x22 -> x20, local copies, waits for them, and re-layouts: 1.9 us -> 5.1 us
  transfers between devices with their start and end apart: 6 -> 2, of which waited for: 4 -> 0; matrix products, arithmetic and copies ran while one was open for 11% -> 4% of each run, Pallas kernels for 0% -> 0%
where the time goes in v1:
time: 113 us; the launch traced here: 112 us
  Pallas kernels  85.6 us (76%)
  local copies, waits for them, and re-layouts  9.71 us (9%)
  matrix products  6.54 us (6%)
  other arithmetic  5.29 us (5%)
  starting transfers between devices  4.32 us (4%)
    pallas_call x1, Pallas kernels, shards(): pl.pallas_call(functools.partial(exchange, experts, parts), out_shape=(ja...  85.6 us
    unnamed x20, local copies, waits for them, and re-layouts  5.1 us
    ppermute x1, starting transfers between devices, extended(): before = lax.ppermute(last, axis, up)  3.04 us
  transfers between devices with their start and end apart: 2, of which 0 were waited for; matrix products, arithmetic and copies ran while one was open for 4% of the time, Pallas kernels for 0%

profile of v1, /device:TPU:0, one launch (start us, length us, event | category | flops | bytes accessed | tf_op | source)
XLA Modules:
  0.0 112.4 jit_solution(8929849359139248863)
XLA Ops:
  0.7 1.7 %fusion.2 = f32[256]{0:T(256)S(1)} fusion(bf16[256,2048]{1,0:T(8,128)(2,1)} %param.14), kind=kLoop, calls=%fused_computation.7 | loop fusion | flops 1572608 | bytes 1049600 | tf_op jit(solution)/shard_map/reduce_sum | solution.py:37
  2.4 2.2 %fusion.33 = f32[256,256]{0,1:T(8,128)S(1)} fusion(bf16[2048,256]{1,0:T(8,128)(2,1)} %param.17, bf16[256,2048]{1,0:T(8,128)(2,1)} %param.14, f32[2048]{0:T(1024)} %param.15, f32[256]{0:T(256)S(1)} %add_rsqrt_fusion), kind=kOutput, calls=%fused_computation.82 | convolution fusion | flops 270532608 | bytes 2368512 | tf_op jit(solution)/shard_map/dot_general | solution.py:340
  4.6 0.7 convolution_convert_fusion
  5.6 0.7 fusion.19
  6.3 3.0 %collective-permute-start = (bf16[128,512]{0,1:T(8,128)(2,1)}, bf16[128,512]{0,1:T(8,128)(2,1)}, u32[]{:S(2)}, u32[]{:S(2)}) collective-permute-start(bf16[128,512]{0,1:T(8,128)(2,1)} %get-tuple-element.16), channel_id=1, source_target_pairs={{0,4},{4,8},{8,12},{12,16},{16,20},{20,24},{24,28},{1,5},{5,9},{9,... | collective-permute-start | bytes 393224 | tf_op jit(solution)/shard_map/ppermute | solution.py:29
  9.4 1.3 %collective-permute-start.1 = (bf16[128,512]{0,1:T(8,128)(2,1)}, bf16[128,512]{0,1:T(8,128)(2,1)}, u32[]{:S(2)}, u32[]{:S(2)}) collective-permute-start(bf16[128,512]{0,1:T(8,128)(2,1)} %get-tuple-element.15), channel_id=1, source_target_pairs={{4,0},{8,4},{12,8},{16,12},{20,16},{24,20},{28,24},{5,1},{9,5},{13... | collective-permute-start | bytes 393224 | tf_op jit(solution)/shard_map/ppermute | solution.py:30
  10.9 1.0 fusion.30
  12.1 0.6 copy.46
  12.7 0.6 copy.47
  13.6 0.7 copy.50.share_ref
  14.3 0.5 fusion.10
  14.8 1.0 pad_maximum_fusion.1
  15.9 0.7 copy_dynamic-update-slice_fusion.2
  16.8 0.8 copy_dynamic-update-slice_fusion.1
  17.5 0.8 copy_dynamic-update-slice_fusion
  18.3 1.7 %fusion.1 = (f32[2,4,2,128]{3,2,1,0:T(2,128)S(1)}, f32[2,4,384,128,2]{3,2,4,1,0:T(8,128)S(1)}) fusion(pred[2,128,384]{1,2,0:T(8,128)(4,1)S(1)} %fusion.10, bf16[2,128,4,2,16]{1,4,3,2,0:T(8,128)(2,1)} %copy.47, bf16[2,128,4,2,16]{1,4,3,2,0:T(8,128)(2,1)} %copy.46, bf16[2,128,4,2,16]{1,4,3,2,0:T(8,128)(2,1)S(1)} %copy.45, ...), kind=kOutput, calls=%fused_computation.6 | convolution fusion | flops 104069120 | bytes 3907584 | tf_op jit(solution)/shard_map/nqgrd,nkgd->ngrqk/dot_general | solution.py:349
  20.1 0.7 fusion
  20.8 0.3 copy-done.2
  21.1 0.9 fusion.7
  22.1 0.4 copy.56
  22.5 1.0 reshape.269.mixed_ref
  23.5 85.6 %shard_map.149 = (bf16[256,512]{1,0:T(8,128)(2,1)}, bf16[128,512]{1,0:T(8,128)(2,1)}) custom-call(bf16[128,2048]{1,0:T(8,128)(2,1)} %x_ref.1, f32[1,2048]{1,0:T(1,128)} %bitcast.60, f32[128,8]{1,0:T(8,128)} %copy.50.share_ref, bf16[256,512]{1,0:T(8,128)(2,1)} %reshape.269.mixed_ref, bf16[2048,512]{1,0:T(8,128)(2,1)} %wo_hbm.1, bf16[2048,512]{1,0:T(8,128)(2,1)} %bitcast.53, ...), custom_call_target="tpu_custom_call" | custom-call | tf_op jit(solution)/shard_map/pallas_call | solution.py:385
  109.2 1.7 %copy.65 = bf16[256,512]{1,0:T(8,128)(2,1)} copy(bf16[256,512]{1,0:T(8,128)(2,1)} %get-tuple-element.33) | data formatting | bytes 524288
  110.8 1.6 %copy.66 = bf16[128,512]{1,0:T(8,128)(2,1)} copy(bf16[128,512]{1,0:T(8,128)(2,1)} %get-tuple-element.34) | data formatting | bytes 262144
  (44 shorter events, 1.2 us)
Async XLA Ops:
  0.6 10.2 %copy-start = (bf16[2048,512]{1,0:T(8,128)(2,1)S(1)}, bf16[2048,512]{1,0:T(8,128)(2,1)}, u32[]{:S(2)}) copy-start(bf16[2048,512]{1,0:T(8,128)(2,1)} %param.16) | copy-start | bytes 6291460
  0.6 4.0 %copy-start.1 = (bf16[256,2048]{1,0:T(8,128)(2,1)S(1)}, bf16[256,2048]{1,0:T(8,128)(2,1)}, u32[]{:S(2)}) copy-start(bf16[256,2048]{1,0:T(8,128)(2,1)} %param.14) | copy-start | bytes 3145732
  0.7 4.0 %copy-start.7 = (f32[2048]{0:T(1024)S(1)}, f32[2048]{0:T(1024)}, u32[]{:S(2)}) copy-start(f32[2048]{0:T(1024)} %param.15) | copy-start | bytes 24580
  0.7 3.9 %copy-start.6 = (bf16[2048,256]{1,0:T(8,128)(2,1)S(1)}, bf16[2048,256]{1,0:T(8,128)(2,1)}, u32[]{:S(2)}) copy-start(bf16[2048,256]{1,0:T(8,128)(2,1)} %param.18) | copy-start | bytes 3145732
  6.3 8.4 %collective-permute-start = (bf16[128,512]{0,1:T(8,128)(2,1)}, bf16[128,512]{0,1:T(8,128)(2,1)}, u32[]{:S(2)}, u32[]{:S(2)}) collective-permute-start(bf16[128,512]{0,1:T(8,128)(2,1)} %get-tuple-element.16), channel_id=1, source_target_pairs={{0,4},{4,8},{8,12},{12,16},{16,20},{20,24},{24,28},{1,5},{5,9},{9,... | collective-permute-start | bytes 393224 | tf_op jit(solution)/shard_map/ppermute | solution.py:29
  9.4 5.4 %collective-permute-start.1 = (bf16[128,512]{0,1:T(8,128)(2,1)}, bf16[128,512]{0,1:T(8,128)(2,1)}, u32[]{:S(2)}, u32[]{:S(2)}) collective-permute-start(bf16[128,512]{0,1:T(8,128)(2,1)} %get-tuple-element.15), channel_id=1, source_target_pairs={{4,0},{8,4},{12,8},{16,12},{20,16},{24,20},{28,24},{5,1},{9,5},{13... | collective-permute-start | bytes 393224 | tf_op jit(solution)/shard_map/ppermute | solution.py:30
  10.8 2.6 %copy-start.5 = (f32[8]{0:T(128)S(1)}, f32[8]{0:T(128)}, u32[]{:S(2)}) copy-start(f32[8]{0:T(128)} %param.20) | copy-start | bytes 100
  10.8 2.6 %copy-start.3 = (f32[128,4]{0,1:T(4,128)S(1)}, f32[128,4]{0,1:T(4,128)}, u32[]{:S(2)}) copy-start(f32[128,4]{0,1:T(4,128)} %param.24) | copy-start | bytes 6148
  10.8 2.7 %copy-start.4 = (s32[128,4]{0,1:T(4,128)S(1)}, s32[128,4]{0,1:T(4,128)}, u32[]{:S(2)}) copy-start(s32[128,4]{0,1:T(4,128)} %param.23) | copy-start | bytes 6148
  20.0 1.1 %copy-start.2 = (bf16[2,384,2,4,64]{1,4,3,0,2:T(8,128)(2,1)S(1)}, bf16[2,384,2,4,64]{1,4,3,0,2:T(8,128)(2,1)}, u32[]{:S(2)}) copy-start(bf16[2,384,2,4,64]{1,4,3,0,2:T(8,128)(2,1)} %copy_dynamic-update-slice_fusion) | copy-start | bytes 2359300

commit v2 on v1

v2 whole, which is shorter than its diff:
```python
import functools

import jax
import jax.numpy as jnp
from jax import lax
from jax.experimental import pallas as pl
from jax.experimental.pallas import tpu as pltpu
from jax.sharding import PartitionSpec as P

HEAD_DIM = 64
TOP_K = 4
WINDOW = 128
GRID_W = 64


EPSILON = 1e-06
LIMIT = 7.0
SLOPE = 1.702
BASE = 10000.0


def normalize(rows, gain):
    values = rows.astype(jnp.float32)
    scaled = values * lax.rsqrt(jnp.mean(values * values, axis=-1, keepdims=True) + EPSILON)
    return (scaled * gain).astype(jnp.bfloat16)


def rotate(values, cosine, sine):
    width = values.shape[1]
    lanes = cosine.shape[1]
    if width < lanes:
        return rotate(jnp.concatenate([values] * (lanes // width), axis=1), cosine, sine)[:, :width]
    spot = lax.broadcasted_iota(jnp.int32, cosine.shape, 1)
    leading = spot % (HEAD_DIM // 2) < HEAD_DIM // 4
    pieces = []
    for start in range(0, width, lanes):
        piece = values[:, start : start + lanes]
        other = jnp.where(
            leading,
            pltpu.roll(piece, lanes - HEAD_DIM // 4, 1),
            pltpu.roll(piece, HEAD_DIM // 4, 1),
        )
        pieces.append(piece * cosine + other * sine)
    return jnp.concatenate(pieces, axis=1)


def activate(gate, up):
    capped = jnp.minimum(gate, LIMIT)
    bounded = jnp.clip(up, -LIMIT, LIMIT)
    return (capped * jax.nn.sigmoid(SLOPE * capped) * (bounded + 1.0)).astype(jnp.bfloat16)


def remote(src, dst, sent, landed, ep, tp):
    return pltpu.make_async_remote_copy(
        src_ref=src,
        dst_ref=dst,
        send_sem=sent,
        recv_sem=landed,
        device_id=(ep, tp),
        device_id_type=pl.DeviceIdType.MESH,
    )


def exchange(
    n,
    t,
    x_ref,
    gain_ref,
    share_ref,
    mixer_ref,
    mixer_gain_ref,
    cosine_ref,
    sine_ref,
    sink_ref,
    wq_hbm,
    wk_hbm,
    wv_hbm,
    wo_hbm,
    wg_hbm,
    wu_hbm,
    wd_hbm,
    mixer_out,
    expert_out,
    tokens,
    hidden,
    heads,
    result,
    returned,
    queries,
    around,
    wq,
    wk,
    wv,
    wo,
    wg,
    wu,
    wd,
    local_sem,
    token_recv,
    far_send,
    near_send,
    core_send,
    hidden_send,
    hidden_recv,
    pass_send,
    pass_recv,
    head_send,
    head_recv,
    edge_send,
    edge_recv,
    result_send,
    result_recv,
):
    ep, tp = lax.axis_index("ep"), lax.axis_index("tp")
    chips = n // 2
    z, core = ep // 2, ep % 2
    step = 1 - 2 * core
    partner = 2 * z + 1 - core
    rows = x_ref.shape[0]
    pair = 2 * rows
    part = wg.shape[1]
    far, near = chips // 2, chips - 1 - chips // 2
    square = t == 4
    direct = (1, 2) if square else tuple(range(1, t))

    def peer(k):
        if not square:
            return lax.rem(tp + k, t)
        return lax.rem(tp + (k // 2) * 2 + (k % 2) * (1 - 2 * (tp % 2)) + t, t)

    def chip(hops):
        return lax.rem(z + hops * step + 2 * chips, chips)

    def block(buffer, index, size):
        return buffer.at[pl.ds(pl.multiple_of(index * size, size), size)]

    loads = [
        pltpu.make_async_copy(a, b, local_sem.at[i])
        for i, (a, b) in enumerate((
            (wq_hbm, wq),
            (wk_hbm, wk),
            (wv_hbm, wv),
            (wg_hbm, wg),
            (wu_hbm, wu),
            (wo_hbm, wo),
            (wd_hbm, wd),
        ))
    ]
    for load in loads:
        load.start()

    barrier = pltpu.get_barrier_semaphore()
    for k in range(1, n):
        pl.semaphore_signal(
            barrier,
            inc=1,
            device_id=(lax.rem(ep + k, n), tp),
            device_id_type=pl.DeviceIdType.MESH,
        )
    for k in range(1, t):
        pl.semaphore_signal(
            barrier,
            inc=1,
            device_id=(ep, peer(k)),
            device_id_type=pl.DeviceIdType.MESH,
        )
    tokens[pl.ds(pl.multiple_of(ep * rows, rows), rows), :] = normalize(x_ref[...], gain_ref[...])
    pl.semaphore_wait(barrier, n + t - 2)

    def token_copy(slot, sent, target):
        piece = block(tokens, slot, rows)
        return remote(piece, piece, sent, token_recv.at[slot], target, tp)

    def forward_far(hop):
        return token_copy(2 * chip(-hop) + core, far_send.at[hop], 2 * chip(1) + core)

    def forward_near(hop):
        return token_copy(2 * chip(hop) + core, near_send.at[hop], 2 * chip(-1) + core)

    def forward_core(hops):
        place = chip(hops)
        return token_copy(2 * place + core, core_send.at[place], partner)

    def token_wait(slot):
        token_copy(slot, core_send.at[0], partner).wait_recv()

    if far > 0:
        forward_far(0).start()
    if near > 0:
        forward_near(0).start()
    forward_core(0).start()

    def head_copy(source, k):
        piece = heads.at[source]
        return remote(piece, piece, head_send.at[k], head_recv.at[source], ep, peer(k))

    def pass_copy(place, way):
        source = peer(2 - way)
        if place is None:
            start, size, index = 0, heads.shape[1] // 2, chips
            buffer = heads.at[source]
        else:
            start, size, index = place * pair, rows, place
            buffer = hidden.at[source]
        piece = buffer.at[pl.ds(pl.multiple_of(start + (1 - way) * size, size), size)]
        return remote(
            piece, piece, pass_send.at[way, index], pass_recv.at[way, index], ep, peer(1 + way)
        )

    def pass_wait(place, way):
        if place is None:
            start, size, index = 0, heads.shape[1] // 2, chips
            buffer = heads.at[peer(3)]
        else:
            start, size, index = place * pair, rows, place
            buffer = hidden.at[peer(3)]
        piece = buffer.at[pl.ds(pl.multiple_of(start + (1 - way) * size, size), size)]
        remote(
            piece, piece, pass_send.at[way, index], pass_recv.at[way, index], ep, peer(1 + way)
        ).wait_recv()

    def hidden_copy(source, place, k):
        piece = block(hidden.at[source], place, pair)
        return remote(
            piece,
            piece,
            hidden_send.at[k, place],
            hidden_recv.at[source, place],
            ep,
            peer(k),
        )

    def hidden_pass(place):
        if square:
            for way in range(2):
                hidden_copy(peer(2 - way), place, 2 - way).wait_recv()
                pass_copy(place, way).start()

    def hidden_wait(place):
        if square:
            for way in range(2):
                pass_wait(place, way)
        else:
            for k in direct:
                hidden_copy(peer(k), place, k).wait_recv()

    def first_half(place):
        token_wait(2 * place + 1 - core)
        inside = pl.ds(pl.multiple_of(place * pair, pair), pair)
        span = min(256, part)
        for start in range(0, part, span):
            cut = slice(start, start + span)
            gate = jnp.dot(tokens[inside, :], wg[:, cut], preferred_element_type=jnp.float32)
            up = jnp.dot(tokens[inside, :], wu[:, cut], preferred_element_type=jnp.float32)
            hidden[tp, inside, cut] = activate(gate, up)
        for k in direct:
            hidden_copy(tp, place, k).start()

    length = mixer_ref.shape[0]
    kept = wk.shape[1]
    normed = normalize(mixer_ref[...], mixer_gain_ref[...])
    cosine, sine = cosine_ref[...], sine_ref[...]
    own = slice(WINDOW, WINDOW + length)
    for load in loads[:3]:
        load.wait()
    keys = jnp.dot(normed, wk[...], preferred_element_type=jnp.float32)
    around[own, 0:kept] = rotate(keys, cosine, sine).astype(jnp.bfloat16)
    around[own, kept:] = jnp.dot(normed, wv[...], preferred_element_type=jnp.float32).astype(
        jnp.bfloat16
    )

    def edge_copy(way):
        source, target = (length, 0) if way == 0 else (WINDOW, WINDOW + length)
        return remote(
            around.at[pl.ds(source, WINDOW)],
            around.at[pl.ds(target, WINDOW)],
            edge_send.at[way],
            edge_recv.at[way],
            lax.rem(ep + (1 if way == 0 else n - 1), n),
            tp,
        )

    for way in range(2):
        edge_copy(way).start()
    turned = jnp.dot(normed, wq[...], preferred_element_type=jnp.float32)
    queries[...] = rotate(turned, cosine, sine).astype(jnp.bfloat16)

    loads[3].wait()
    loads[4].wait()
    first_half(z)

    def attend(number, carry):
        inside = pl.ds(pl.multiple_of(number * WINDOW, WINDOW), WINDOW)
        seen = pl.ds(pl.multiple_of(number * WINDOW, WINDOW), 3 * WINDOW)
        shape = (WINDOW, 3 * WINDOW)
        line = lax.broadcasted_iota(jnp.int32, shape, 0)
        key = lax.broadcasted_iota(jnp.int32, shape, 1)
        place = ep * length + (number - 1) * WINDOW + key
        allowed = (key >= line) & (key <= line + 2 * WINDOW) & (place >= 0) & (place < n * length)
        group = queries.shape[1] // kept
        allowed = jnp.concatenate([allowed] * group, axis=0)
        for head in range(kept // HEAD_DIM):
            first = head * group
            query = jnp.concatenate(
                [
                    queries[inside, (first + r) * HEAD_DIM : (first + r + 1) * HEAD_DIM]
                    for r in range(group)
                ],
                axis=0,
            )
            sinks = jnp.concatenate(
                [
                    jnp.broadcast_to(sink_ref[:, first + r : first + r + 1], (WINDOW, 1))
                    for r in range(group)
                ],
                axis=0,
            )
            near_keys = around[seen, head * HEAD_DIM : (head + 1) * HEAD_DIM]
            near_values = around[seen, kept + head * HEAD_DIM : kept + (head + 1) * HEAD_DIM]
            scores = lax.dot_general(
                query,
                near_keys,
                (((1,), (1,)), ((), ())),
                preferred_element_type=jnp.float32,
            ) * HEAD_DIM ** (-0.5)
            scores = jnp.where(allowed, scores, -1e30)
            top = jnp.maximum(jnp.max(scores, axis=-1, keepdims=True), sinks)
            weights = jnp.exp(scores - top)
            denominator = jnp.sum(weights, axis=-1, keepdims=True) + jnp.exp(sinks - top)
            shares = (weights * (1.0 / denominator)).astype(jnp.bfloat16)
            mixed = jnp.dot(shares, near_values, preferred_element_type=jnp.float32)
            mixed = mixed.astype(jnp.bfloat16)
            heads[tp, inside, first * HEAD_DIM : (first + group) * HEAD_DIM] = jnp.concatenate(
                [mixed[r * WINDOW : (r + 1) * WINDOW] for r in range(group)], axis=1
            )
        return carry

    def attention():
        for way in range(2):
            edge_copy(way).wait_recv()
        lax.fori_loop(0, length // WINDOW, attend, 0)
        for k in direct:
            head_copy(tp, k).start()

    for hop in range(1, far + 1):
        token_wait(2 * chip(-hop) + core)
        if hop < far:
            forward_far(hop).start()
        forward_core(-hop).start()
        if hop <= near:
            token_wait(2 * chip(hop) + core)
            if hop < near:
                forward_near(hop).start()
            forward_core(hop).start()
            if hop == 1:
                attention()

            def both(k, carry, hop=hop):
                first_half(chip((2 * k - 1) * hop))
                return carry

            lax.fori_loop(0, 2, both, 0)
            if hop == 1 and square:
                hidden_pass(z)
                for way in range(2):
                    head_copy(peer(2 - way), 2 - way).wait_recv()
                    pass_copy(None, way).start()
        else:
            first_half(chip(-hop))

    def place_of(i):
        return chip((i + 1) // 2 * (2 * ((i + 1) % 2) - 1))

    def pass_on(i, carry):
        hidden_pass(place_of(i))
        return carry

    lax.fori_loop(1, chips - 1, pass_on, 0)

    loads[5].wait()
    if square:
        for way in range(2):
            pass_wait(None, way)
    else:
        for k in direct:
            head_copy(peer(k), k).wait_recv()
    total = jnp.dot(heads[0], wo[0:part, :], preferred_element_type=jnp.float32)
    for k in range(1, t):
        total += jnp.dot(
            heads[k], wo[k * part : (k + 1) * part, :], preferred_element_type=jnp.float32
        )
    mixer_out[...] = total.astype(jnp.bfloat16)

    loads[6].wait()

    def result_copy(source, owner):
        return remote(
            block(result, owner, rows),
            returned.at[source],
            result_send.at[owner],
            result_recv.at[source],
            owner,
            tp,
        )

    def second_half(i, carry):
        place = place_of(i)
        inside = pl.ds(pl.multiple_of(place * pair, pair), pair)
        hidden_wait(place)
        total = jnp.dot(hidden[0, inside, :], wd[0:part, :], preferred_element_type=jnp.float32)
        for k in range(1, t):
            total += jnp.dot(
                hidden[k, inside, :],
                wd[k * part : (k + 1) * part, :],
                preferred_element_type=jnp.float32,
            )
        result[inside, :] = total.astype(jnp.bfloat16)

        @pl.when(i == 0)
        def _():
            result_copy(ep, partner).start()
            returned[ep] = result[pl.ds(pl.multiple_of(ep * rows, rows), rows), :]

        @pl.when(i > 0)
        def _():
            result_copy(ep, 2 * place + core).start()
            result_copy(ep, 2 * place + 1 - core).start()

        return carry

    lax.fori_loop(0, chips - 2, second_half, 0)
    hidden_pass(place_of(chips - 1))
    lax.fori_loop(chips - 2, chips, second_half, 0)

    for k in range(1, n):
        other = lax.rem(ep + k, n)
        result_copy(other, other).wait_recv()
    total = returned[0].astype(jnp.float32) * share_ref[:, 0:1]
    for e in range(1, n):
        total += returned[e].astype(jnp.float32) * share_ref[:, e : e + 1]
    expert_out[...] = total.astype(jnp.bfloat16)

    for hop in range(far):
        forward_far(hop).wait_send()
    for hop in range(near):
        forward_near(hop).wait_send()
    for hop in range(chips):
        forward_core(hop).wait_send()
    for way in range(2):
        edge_copy(way).wait_send()
        if square:
            pass_copy(None, way).wait_send()
            for place in range(chips):
                pass_copy(place, way).wait_send()
    for k in direct:
        head_copy(tp, k).wait_send()
        for place in range(chips):
            hidden_copy(tp, place, k).wait_send()
    for k in range(1, n):
        result_copy(ep, lax.rem(ep + k, n)).wait_send()


def shards(
    mixer_input,
    mixer_gain,
    query_weight,
    key_weight,
    value_weight,
    output_weight,
    sink_logit,
    expert_input,
    expert_gain,
    routes,
    route_logits,
    gate_weight,
    up_weight,
    down_weight,
):
    tokens = mixer_input.shape[0]
    lanes = 2 * HEAD_DIM
    quarter = HEAD_DIM // 4
    spot = jnp.arange(lanes, dtype=jnp.int32)[None, :]
    place = (lax.axis_index("ep") * tokens + jnp.arange(tokens, dtype=jnp.int32))[:, None]
    frequency = BASE ** (-(spot % quarter).astype(jnp.float32) / quarter)
    by_row = spot % HEAD_DIM < HEAD_DIM // 2
    turn = jnp.where(by_row, place // GRID_W, place % GRID_W).astype(jnp.float32) * frequency
    cosine = jnp.cos(turn)
    sine = jnp.sin(turn) * jnp.where(spot % (HEAD_DIM // 2) < quarter, -1.0, 1.0)
    experts = lax.axis_size("ep")
    parts = lax.axis_size("tp")
    rows_here, width = expert_input.shape
    part = gate_weight.shape[2]
    chances = jax.nn.softmax(route_logits, axis=-1)
    named = routes[:, :, None] == jnp.arange(experts, dtype=jnp.int32)[None, None, :]
    expert_share = jnp.sum(jnp.where(named, chances[:, :, None], 0.0), axis=1)
    vmem = pl.BlockSpec(memory_space=pltpu.VMEM)
    anywhere = pl.BlockSpec(memory_space=pl.ANY)
    chips = experts // 2
    dma = pltpu.SemaphoreType.DMA
    columns = down_weight.shape[2]
    return pl.pallas_call(
        functools.partial(exchange, experts, parts),
        out_shape=(
            jax.ShapeDtypeStruct((tokens, output_weight.shape[1]), jnp.bfloat16),
            jax.ShapeDtypeStruct((rows_here, columns), jnp.bfloat16),
        ),
        in_specs=[vmem] * 8 + [anywhere] * 7,
        out_specs=(vmem, vmem),
        scratch_shapes=[
            pltpu.VMEM((experts * rows_here, width), jnp.bfloat16),
            pltpu.VMEM((parts, experts * rows_here, part), jnp.bfloat16),
            pltpu.VMEM((parts, tokens, query_weight.shape[1]), jnp.bfloat16),
            pltpu.VMEM((experts * rows_here, columns), jnp.bfloat16),
            pltpu.VMEM((experts, rows_here, columns), jnp.bfloat16),
            pltpu.VMEM((tokens, query_weight.shape[1]), jnp.bfloat16),
            pltpu.VMEM((tokens + 2 * WINDOW, 2 * key_weight.shape[1]), jnp.bfloat16),
            pltpu.VMEM(query_weight.shape, jnp.bfloat16),
            pltpu.VMEM(key_weight.shape, jnp.bfloat16),
            pltpu.VMEM(value_weight.shape, jnp.bfloat16),
            pltpu.VMEM(output_weight.shape, jnp.bfloat16),
            pltpu.VMEM(gate_weight.shape[1:], jnp.bfloat16),
            pltpu.VMEM(up_weight.shape[1:], jnp.bfloat16),
            pltpu.VMEM(down_weight.shape[1:], jnp.bfloat16),
            dma((7,)),
            dma((experts,)),
            dma((chips,)),
            dma((chips,)),
            dma((chips,)),
            dma((parts, chips)),
            dma((parts, chips)),
            dma((2, chips + 1)),
            dma((2, chips + 1)),
            dma((parts,)),
            dma((parts,)),
            dma((2,)),
            dma((2,)),
            dma((experts,)),
            dma((experts,)),
        ],
        compiler_params=pltpu.CompilerParams(
            collective_id=0, has_side_effects=True, vmem_limit_bytes=60 * 1024 * 1024
        ),
    )(
        expert_input,
        expert_gain.reshape(1, -1),
        expert_share,
        mixer_input,
        mixer_gain.reshape(1, -1),
        cosine,
        sine,
        sink_logit.reshape(1, -1),
        query_weight,
        key_weight,
        value_weight,
        output_weight,
        gate_weight[0],
        up_weight[0],
        down_weight[0],
    )


def solution(mesh):
    return jax.shard_map(
        shards,
        mesh=mesh,
        in_specs=(
            P("ep", None),
            P(),
            P(None, "tp"),
            P(None, "tp"),
            P(None, "tp"),
            P(None, "tp"),
            P("tp"),
            P("ep", None),
            P(),
            P("ep", None),
            P("ep", None),
            P("ep", None, "tp"),
            P("ep", None, "tp"),
            P("ep", None, "tp"),
        ),
        out_specs=(P("ep", "tp"), P("ep", "tp")),
        check_vma=False,
    )
```

time: 113 us -> 111 us (0.982)
  Pallas kernels: 85.6 us -> 102 us
  matrix products: 6.54 us -> 0 us
  local copies, waits for them, and re-layouts: 9.71 us -> 3.96 us
  starting transfers between devices: 4.32 us -> 0 us
  other arithmetic: 5.29 us -> 4.07 us
    pallas_call x1, Pallas kernels: 85.6 us -> 102 us  [shards(): pl.pallas_call(functools.partial(exchange, experts, parts), out_shape=(ja...]
    dot_general x5 -> x0, matrix products: 6.54 us -> none  [the longest x1 2.21 us: shards(): jnp.dot(normed, key_weight, preferred_element_type=jnp.float32)]
    ppermute x2 -> x0, starting transfers between devices: 4.32 us -> none  [the longest x1 3.04 us: extended(): before = lax.ppermute(last, axis, up)]
    reduce_sum x2 -> x0, other arithmetic: 2.33 us -> none  [the longest x1 1.66 us: normalize(): jnp.mean(values * values, axis=-1, keepdims=True) + EPSILON]
    concatenate x9 -> x0, local copies, waits for them, and re-layouts: 2.18 us -> none  [the longest x8 1.39 us: axial_rope(): jnp.concatenate([turn(row_part, jnp.cos(row_angle), jnp.sin(row_angle)),...]
    unnamed x20 -> x2, local copies, waits for them, and re-layouts: 5.1 us -> 3.24 us
    concatenate x3 -> x0, other arithmetic: 1.76 us -> none  [the longest x1 1.03 us: extended(): shard = jnp.concatenate([before, shard, after], axis=dim)]
    reshape x2 -> x0, local copies, waits for them, and re-layouts: 1.43 us -> none  [shards(): mixed = mixed.astype(jnp.bfloat16).reshape(tokens, query_heads * HEAD_DIM)]
  transfers between devices with their start and end apart: 2 -> 0, of which waited for: 0 -> 0; matrix products, arithmetic and copies ran while one was open for 4% -> 0% of each run, Pallas kernels for 0% -> 0%
where the time goes in v2:
time: 111 us
  Pallas kernels  102 us (92%)
  other arithmetic  4.07 us (4%)
  local copies, waits for them, and re-layouts  3.96 us (4%)
    pallas_call x1, Pallas kernels, shards(): pl.pallas_call(functools.partial(exchange, experts, parts), out_shape=(ja...  102 us
    unnamed x2, local copies, waits for them, and re-layouts  3.24 us

profile of v2, /device:TPU:0, one launch (start us, length us, event | category | flops | bytes accessed | tf_op | source)
XLA Modules:
  0.0 110.9 jit_solution(10300028031937659614)
XLA Ops:
  0.6 0.7 reduce_max.9
  1.3 0.7 fusion.2
  2.0 0.7 fusion.1
  2.8 0.7 select_reduce_fusion
  3.5 0.7 copy.18.share_ref
  4.2 1.3 %sine_multiply_fusion = (f32[256,128]{1,0:T(8,128)}, f32[256,128]{1,0:T(8,128)}) fusion(f32[128]{0:T(128)S(1)} %get-tuple-element.6, f32[128]{0:T(128)S(1)} %get-tuple-element.7, s32[256]{0:T(256)S(1)} %get-tuple-element.4, s32[256]{0:T(256)S(1)} %get-tuple-element.5, pred[128]{0:T(512)(128)(4,1)S(1)} %fusion.4), kind=kLoop, calls=%fused_computation | loop fusion | flops 131072 | bytes 265344 | tf_op jit(solution)/shard_map/mul | solution.py:488
  5.4 102.2 %shard_map.149 = (bf16[256,512]{1,0:T(8,128)(2,1)}, bf16[128,512]{1,0:T(8,128)(2,1)}) custom-call(bf16[128,2048]{1,0:T(8,128)(2,1)} %x_ref.1, f32[1,2048]{1,0:T(1,128)} %bitcast.9, f32[128,8]{1,0:T(8,128)} %copy.18.share_ref, bf16[256,2048]{1,0:T(8,128)(2,1)} %mixer_ref.1, f32[1,2048]{1,0:T(1,128)} %bitcast.10, f32[256,128]{1,0:T(8,128)} %get-tuple-element.3.cosine_ref, ...), custom_call_target="tpu_custom_call" | custom-call | tf_op jit(solution)/shard_map/pallas_call | solution.py:501
  107.6 1.7 %copy.21 = bf16[256,512]{1,0:T(8,128)(2,1)} copy(bf16[256,512]{1,0:T(8,128)(2,1)} %get-tuple-element.10) | data formatting | bytes 524288
  109.3 1.6 %copy.22 = bf16[128,512]{1,0:T(8,128)(2,1)} copy(bf16[128,512]{1,0:T(8,128)(2,1)} %get-tuple-element.11) | data formatting | bytes 262144
  (3 shorter events, 0.0 us)
